TPU v7x, 32 devices: a whole 2x2x4 slice. The times are simulated.
32 devices in a mesh: sp: 8 (over z, x), tp: 4 (over y, core).
Axes of the slice: x: 2, y: 2, z: 4, core: 2. Of those that a mesh axis runs over, the one named last changes fastest.
Arguments:
- stream: bfloat16 [4096, 2048], P(('sp', 'tp')), may hold values from -6 to 6
- queries: bfloat16 [4096, 512], P('sp', 'tp'), may hold values from -6 to 6
- key_rows: bfloat16 [4096, 512], P('sp', 'tp'), may hold values from -6 to 6
- values: bfloat16 [4096, 1024], P('sp', 'tp'), may hold values from -6 to 6
- out_gate: bfloat16 [4096, 1024], P('sp', 'tp'), may hold values from -6 to 6
- fwd_decay: float32 [4096, 512], P('sp', 'tp'), may hold values from -14 to 14
- bwd_decay: float32 [4096, 512], P('sp', 'tp'), may hold values from -14 to 14
- head_gain: float32 [1024], P('tp'), may hold values from 0.1 to 1.9
- out_proj: bfloat16 [1024, 2048], replicated, may hold values from -0.1875 to 0.1875
- mix_gain: float32 [2048], replicated, may hold values from 0.1 to 1.9
- ffn_gain: float32 [2048], replicated, may hold values from 0.1 to 1.9
- moe_gain: float32 [2048], replicated, may hold values from 0.1 to 1.9
- routes: int32 [4096, 2], P(('sp', 'tp')), may hold values from 0 to 7, all different within a row; in each aligned block of 128 rows (0 to 127, 128 to 255, ...) at most 48 rows name the same one
- route_weight: float32 [4096, 2], P(('sp', 'tp')), may hold values from 0.25 to 2.5
- expert_gate: bfloat16 [8, 2048, 1024], P('sp', None, 'tp'), may hold values from -0.125 to 0.125
- expert_up: bfloat16 [8, 2048, 1024], P('sp', None, 'tp'), may hold values from -0.125 to 0.125
- expert_down: bfloat16 [8, 1024, 2048], P('sp', 'tp'), may hold values from -0.1875 to 0.1875
- shared_gate: bfloat16 [2048, 512], P(None, 'tp'), may hold values from -0.125 to 0.125
- shared_up: bfloat16 [2048, 512], P(None, 'tp'), may hold values from -0.125 to 0.125
- shared_down: bfloat16 [512, 2048], P('tp'), may hold values from -0.25 to 0.25
Outputs:
- updated: bfloat16 [4096, 2048], P(('sp', 'tp'))
Inputs may be any that keep to these rules, and one draw needn't show every extreme that they name: `routes`: each row names 2 different experts. Among the rows of one device no expert is named more than 48 times, and in every draw some device names some expert exactly 48 times.
All inputs are finite; a program needn't handle non-finite values.
Results may differ from a plain program's by a relative error of at most 0.023.
Values may be sent and summed in bfloat16 or wider, within the bound.
A program may use at most 128 MiB of HBM per device.

v0:
```python
import jax
import jax.numpy as jnp
from jax import lax
from jax.sharding import PartitionSpec as P

KEY_CHANNELS = 64
DV = 128
BLK = 64
TOPK = 2
EPS = 1e-06
GATE_NORM = 16.0
ROPE_BASE = 10000.0
TOP_PRECISION = lax.Precision.HIGHEST


def carried_in(fwd_summary, bwd_summary, axis):
    count = lax.axis_size(axis)
    place = lax.axis_index(axis)
    decays = jnp.stack([fwd_summary[0], bwd_summary[0]])
    states = jnp.stack([fwd_summary[1], bwd_summary[1]])
    width = states.shape[-1]
    packed = jnp.concatenate([states.reshape(-1, width), decays.reshape(-1, width)], axis=0).astype(
        jnp.bfloat16
    )
    gathered = lax.all_gather(packed, axis).astype(jnp.float32)
    state_rows = states.size // width
    all_states = gathered[:, :state_rows].reshape((count,) + states.shape)
    all_decays = gathered[:, state_rows:].reshape((count,) + decays.shape)
    fwd = jnp.zeros_like(states[0])
    bwd = jnp.zeros_like(states[0])
    for step in range(count):
        fwd = jnp.where(
            step < place, fwd * all_decays[step, 0][:, :, None] + all_states[step, 0], fwd
        )
        source = count - 1 - step
        bwd = jnp.where(
            source > place, bwd * all_decays[source, 1][:, :, None] + all_states[source, 1], bwd
        )
    return (fwd, bwd)


def normalize(tensor):
    return tensor * lax.rsqrt(jnp.mean(tensor * tensor, axis=-1, keepdims=True) + EPS)


def rotate(tensor, positions):
    half_width = tensor.shape[-1] // 2
    frequency = ROPE_BASE ** (-jnp.arange(half_width, dtype=jnp.float32) / half_width)
    angles = positions[:, None] * frequency[None, :]
    cosine = jnp.cos(angles)[:, None, :]
    sine_part = jnp.sin(angles)[:, None, :]
    front_half = tensor[..., :half_width]
    back_half = tensor[..., half_width:]
    return jnp.concatenate(
        [front_half * cosine - back_half * sine_part, front_half * sine_part + back_half * cosine],
        axis=-1,
    )


def blockwise(query_rows, key_data, value_matrix, log_decay, start_state):
    length, head_count, key_width = query_rows.shape
    value_width = value_matrix.shape[-1]
    block_count = length // BLK
    query_blocks = query_rows.reshape(block_count, BLK, head_count, key_width)
    key_blocks = key_data.reshape(block_count, BLK, head_count, key_width)
    value_blocks = value_matrix.reshape(block_count, BLK, head_count, value_width)
    cumul = jnp.cumsum(log_decay.reshape(block_count, BLK, head_count, key_width), axis=1)
    middle = cumul[:, BLK // 2 - 1 : BLK // 2]
    query_scaled = query_blocks * jnp.exp(cumul - middle)
    key_scaled = key_blocks * jnp.exp(middle - cumul)
    scores = jnp.einsum("nthk,nshk->nhts", query_scaled, key_scaled, precision=TOP_PRECISION)
    lower_mask = jnp.arange(BLK)[:, None] >= jnp.arange(BLK)[None, :]
    scores = jnp.where(lower_mask, scores, 0.0)
    within = jnp.einsum("nhts,nshv->nthv", scores, value_blocks, precision=TOP_PRECISION)
    last_cumul = cumul[:, -1:]
    query_in = query_blocks * jnp.exp(cumul)
    key_out = key_blocks * jnp.exp(last_cumul - cumul)
    block_decay = jnp.exp(last_cumul[:, 0])

    def advance(carried_state, pieces):
        query_segment, key_segment, value_segment, decay_segment = pieces
        across_blocks = jnp.einsum(
            "asu,sun->asn", query_segment, carried_state, precision=TOP_PRECISION
        )
        carried_state = carried_state * decay_segment[:, :, None] + jnp.einsum(
            "jco,jcm->com", key_segment, value_segment, precision=TOP_PRECISION
        )
        return (carried_state, across_blocks)

    final_state, across_blocks = lax.scan(
        advance, start_state, (query_in, key_out, value_blocks, block_decay), unroll=block_count
    )
    return ((within + across_blocks).reshape(length, head_count, value_width), final_state)


def summarize(key_data, value_matrix, log_decay):
    cumul = jnp.cumsum(log_decay, axis=0)
    grand_total = cumul[-1]
    weighted_rows = key_data * jnp.exp(grand_total[None] - cumul)
    return (
        jnp.exp(grand_total),
        jnp.einsum("jco,jcm->com", weighted_rows, value_matrix, precision=TOP_PRECISION),
    )


def feed_forward(row_data, gate_parts, up_parts, down_mat):
    groups, _, width = gate_parts.shape
    total = jnp.zeros((row_data.shape[0], down_mat.shape[1]), jnp.float32)
    for group in range(groups):
        hidden = (
            jax.nn.silu(jnp.dot(row_data, gate_parts[group], preferred_element_type=jnp.float32))
            * jnp.dot(row_data, up_parts[group], preferred_element_type=jnp.float32)
        ).astype(jnp.bfloat16)
        total = total + jnp.dot(
            hidden,
            down_mat[group * width : (group + 1) * width],
            preferred_element_type=jnp.float32,
        )
    return total


def slot_map(route_block, experts, capacity):
    tokens, choices = route_block.shape
    flat_ids = route_block.reshape(-1)
    total = flat_ids.shape[0]
    onehot = (flat_ids[:, None] == jnp.arange(experts, dtype=jnp.int32)[None, :]).astype(
        jnp.bfloat16
    )
    earlier = (jnp.arange(total)[:, None] > jnp.arange(total)[None, :]).astype(jnp.bfloat16)
    before = jnp.dot(earlier, onehot, preferred_element_type=jnp.float32)
    slot_ids = jnp.sum(before * onehot.astype(jnp.float32), axis=1).astype(jnp.int32)
    return (flat_ids * capacity + slot_ids).reshape(tokens, choices)


def body(
    stream,
    queries,
    key_rows,
    values,
    out_gate,
    fwd_decay,
    bwd_decay,
    head_gain,
    out_proj,
    mix_gain,
    ffn_gain,
    moe_gain,
    routes,
    route_weight,
    expert_gate,
    expert_up,
    expert_down,
    shared_gate,
    shared_up,
    shared_down,
):
    tokens_here = stream.shape[0]
    span_rows = queries.shape[0]
    heads_here = queries.shape[1] // KEY_CHANNELS
    experts = lax.axis_size("sp")
    capacity = max(2, 3 * tokens_here * TOPK // (2 * experts))
    gate_parts = lax.all_gather(expert_gate[0], "tp")
    up_parts = lax.all_gather(expert_up[0], "tp")
    down_mat = lax.all_gather(expert_down[0], "tp", axis=0, tiled=True)
    shared_gate_parts = lax.all_gather(shared_gate, "tp")
    shared_up_parts = lax.all_gather(shared_up, "tp")
    shared_down_mat = lax.all_gather(shared_down, "tp", axis=0, tiled=True)
    rows_of = slot_map(routes, experts, capacity)
    slots = jnp.arange(experts * capacity, dtype=jnp.int32)
    taken = rows_of[:, :, None] == slots[None, None, :]
    pick = jnp.any(taken, axis=1).astype(jnp.bfloat16)
    weights = jnp.sum(jnp.where(taken, route_weight[:, :, None], 0.0), axis=1)
    weights_high = weights.astype(jnp.bfloat16)
    weights_low = (weights - weights_high.astype(jnp.float32)).astype(jnp.bfloat16)
    offset = lax.axis_index("sp") * span_rows
    positions = (offset + jnp.arange(span_rows, dtype=jnp.int32)).astype(jnp.float32)
    query_rows = rotate(
        queries.astype(jnp.float32).reshape(span_rows, heads_here, KEY_CHANNELS)
        * KEY_CHANNELS ** (-0.5),
        positions,
    )
    key_data = rotate(
        key_rows.astype(jnp.float32).reshape(span_rows, heads_here, KEY_CHANNELS), positions
    )
    value_matrix = values.astype(jnp.float32).reshape(span_rows, heads_here, DV)
    fwd_log = jax.nn.log_sigmoid(fwd_decay).reshape(span_rows, heads_here, KEY_CHANNELS) / GATE_NORM
    bwd_log = (
        jax.nn.log_sigmoid(bwd_decay[::-1]).reshape(span_rows, heads_here, KEY_CHANNELS) / GATE_NORM
    )
    query_back = query_rows[::-1]
    key_back = key_data[::-1]
    value_back = value_matrix[::-1]
    fwd_summary = summarize(key_data, value_matrix, fwd_log)
    bwd_summary = summarize(key_back, value_back, bwd_log)
    fwd_carry, bwd_carry = carried_in(fwd_summary, bwd_summary, "sp")
    fwd_out, _ = blockwise(query_rows, key_data, value_matrix, fwd_log, fwd_carry)
    bwd_out, _ = blockwise(query_back, key_back, value_back, bwd_log, bwd_carry)
    combined = normalize(fwd_out + bwd_out[::-1]) * head_gain.reshape(heads_here, DV)
    head_mixed = (
        combined.reshape(span_rows, -1) * jax.nn.silu(out_gate.astype(jnp.float32))
    ).astype(jnp.bfloat16)
    mixed_out = lax.all_to_all(head_mixed, "tp", split_axis=0, concat_axis=1, tiled=True)
    projected = jnp.dot(mixed_out, out_proj, preferred_element_type=jnp.float32)
    residual = (stream.astype(jnp.float32) + normalize(projected) * mix_gain).astype(jnp.bfloat16)
    normed = (normalize(residual.astype(jnp.float32)) * ffn_gain).astype(jnp.bfloat16)
    model_width = normed.shape[1]
    outgoing = lax.dot_general(
        pick, normed, (((0,), (0,)), ((), ())), preferred_element_type=jnp.float32
    ).astype(jnp.bfloat16)
    arrived = lax.all_to_all(
        outgoing.reshape(experts, capacity, model_width),
        "sp",
        split_axis=0,
        concat_axis=0,
        tiled=True,
    )
    shared_sum = feed_forward(normed, shared_gate_parts, shared_up_parts, shared_down_mat)
    routed_done = feed_forward(
        arrived.reshape(experts * capacity, model_width), gate_parts, up_parts, down_mat
    ).astype(jnp.bfloat16)
    routed_back = lax.all_to_all(
        routed_done.reshape(experts, capacity, model_width),
        "sp",
        split_axis=0,
        concat_axis=0,
        tiled=True,
    ).reshape(experts * capacity, model_width)
    mixture = (
        shared_sum
        + jnp.dot(weights_high, routed_back, preferred_element_type=jnp.float32)
        + jnp.dot(weights_low, routed_back, preferred_element_type=jnp.float32)
    )
    return (residual.astype(jnp.float32) + normalize(mixture) * moe_gain).astype(jnp.bfloat16)


def solution(mesh):
    return jax.shard_map(
        body,
        mesh=mesh,
        in_specs=(
            P(("sp", "tp"), None),
            P("sp", "tp"),
            P("sp", "tp"),
            P("sp", "tp"),
            P("sp", "tp"),
            P("sp", "tp"),
            P("sp", "tp"),
            P("tp"),
            P(),
            P(),
            P(),
            P(),
            P(("sp", "tp"), None),
            P(("sp", "tp"), None),
            P("sp", None, "tp"),
            P("sp", None, "tp"),
            P("sp", "tp", None),
            P(None, "tp"),
            P(None, "tp"),
            P("tp", None),
        ),
        out_specs=P(("sp", "tp"), None),
        check_vma=False,
    )
```

profile of v0, /device:TPU:0, one launch (start us, length us, event | category | flops | bytes accessed | tf_op | source)
XLA Modules:
  0.0 286.0 jit_solution(18210130579138707508)
XLA Ops:
  11.9 2.4 reduce-window.14
  17.0 2.4 reduce-window.16
  22.3 3.8 %rev.17 = f32[512,2,128]{0,2,1:T(8,128)S(1)} reverse(f32[512,2,128]{0,2,1:T(8,128)} %bitcast.614), dimensions={0} | reverse | bytes 1048576 | tf_op jit(solution)/shard_map/rev | solution.py:192
  29.0 33.1 %all_gather.28 = bf16[8,258,128]{2,1,0:T(8,128)(2,1)S(1)} all-gather(bf16[1,258,128]{2,1,0:T(8,128)(2,1)S(1)} %pad_maximum_fusion.2), channel_id=1, replica_groups=mesh['sp'=8,'tp'=4] {'sp'}, dimensions={0}, use_global_device_ids=true | all-gather | bytes 594432 | tf_op jit(solution)/shard_map/all_gather | solution.py:25
  71.4 3.3 %rev.18 = f32[512,2,64]{0,2,1:T(8,128)} reverse(f32[512,2,64]{0,2,1:T(8,128)} %get-tuple-element.71), dimensions={0} | reverse | bytes 524288 | tf_op jit(solution)/shard_map/rev | solution.py:190
  75.1 13.0 %fusion.218 = f32[8,64,2,64]{3,0,1,2:T(8,128)S(1)} fusion(f32[8,64,2,64]{3,0,1,2:T(8,128)S(1)} %copy.390), kind=kOutput, calls=%fused_computation.394 | output fusion | flops 4128768 | bytes 524288 | tf_op jit(solution)/shard_map/jit(cumsum)/reduce_window_sum | solution.py:67
  95.8 1.6 fusion.215
  99.2 1.6 fusion.216
  107.6 2.2 copy_multiply_fusion.1
  138.2 1.7 fusion.11
  140.9 1.7 fusion.10
  143.6 1.7 fusion.9
  146.5 1.7 fusion
  150.6 3.4 %all-to-all-start = ((bf16[4,128,256]{2,1,0:T(8,128)(2,1)}), bf16[4,128,256]{2,1,0:T(8,128)(2,1)S(1)}, u32[]{:S(2)}, u32[]{:S(2)}) async-start(bf16[4,128,256]{2,1,0:T(8,128)(2,1)} %bitcast.143), calls=%async_computation | async-start | bytes 524288 | tf_op jit(solution)/shard_map/all_to_all | solution.py:202
  155.5 4.6 %all-to-all-done = bf16[4,128,256]{2,1,0:T(8,128)(2,1)S(1)} async-done(((bf16[4,128,256]{2,1,0:T(8,128)(2,1)}), bf16[4,128,256]{2,1,0:T(8,128)(2,1)S(1)}, u32[]{:S(2)}, u32[]{:S(2)}) %all-to-all-start) | async-done | bytes 262176 | tf_op jit(solution)/shard_map/all_to_all | solution.py:202
  160.2 3.1 %multiply_reduce_fusion.1 = (f32[128]{0:T(128)S(1)}, f32[128,2048]{1,0:T(8,128)S(1)}) fusion(bf16[128,1024]{0,1:T(8,128)(2,1)S(1)} %bitcast.616, bf16[1024,2048]{1,0:T(8,128)(2,1)} %param.28), kind=kOutput, calls=%fused_computation.110 | convolution fusion | flops 537395072 | bytes 5505536 | tf_op jit(solution)/shard_map/dot_general | solution.py:203
  164.0 1.8 convolution_convert_fusion
  165.8 5.6 %all-to-all-start.1 = ((bf16[8,48,2048]{2,1,0:T(8,128)(2,1)}), bf16[8,48,2048]{2,1,0:T(8,128)(2,1)S(1)}, u32[]{:S(2)}, u32[]{:S(2)}) async-start(bf16[8,48,2048]{2,1,0:T(8,128)(2,1)} %bitcast.608), calls=%async_computation.1 | async-start | bytes 3145728 | tf_op jit(solution)/shard_map/all_to_all | solution.py:210
  172.0 36.1 %all-to-all-done.1 = bf16[8,48,2048]{2,1,0:T(8,128)(2,1)S(1)} async-done(((bf16[8,48,2048]{2,1,0:T(8,128)(2,1)}), bf16[8,48,2048]{2,1,0:T(8,128)(2,1)S(1)}, u32[]{:S(2)}, u32[]{:S(2)}) %all-to-all-start.1) | async-done | bytes 1572896 | tf_op jit(solution)/shard_map/all_to_all | solution.py:210
  208.1 1.9 fusion.39
  211.9 5.0 %fusion.7 = f32[384,2048]{1,0:T(8,128)} fusion(bf16[384,2048]{1,0:T(8,128)(2,1)S(1)} %bitcast.600, bf16[1,1024,2048]{2,1,0:T(8,128)(2,1)} %all-gather.20.cloned.1.call-done, bf16[4,2048,256]{2,1,0:T(8,128)(2,1)} %all-gather.14.cloned.1.call-done, f32[384,256]{1,0:T(8,128)S(1)} %fusion.39), kind=kOutput, calls=%fused_computation.25 | convolution fusion | flops 805896192 | bytes 7208960 | tf_op jit(solution)/shard_map/dot_general | solution.py:114
  216.8 1.8 fusion.37
  218.6 5.0 %fusion.8 = f32[384,2048]{1,0:T(8,128)} fusion(bf16[384,2048]{1,0:T(8,128)(2,1)S(1)} %bitcast.602, bf16[1,1024,2048]{2,1,0:T(8,128)(2,1)} %all-gather.20.cloned.1.call-done, bf16[4,2048,256]{2,1,0:T(8,128)(2,1)} %all-gather.14.cloned.1.call-done, f32[384,256]{1,0:T(8,128)S(1)} %fusion.40), kind=kOutput, calls=%fused_computation.26 | convolution fusion | flops 805896192 | bytes 7208960 | tf_op jit(solution)/shard_map/dot_general | solution.py:114
  223.7 5.0 %fusion.6 = f32[384,2048]{1,0:T(8,128)} fusion(bf16[384,2048]{1,0:T(8,128)(2,1)S(1)} %bitcast.603, bf16[1,1024,2048]{2,1,0:T(8,128)(2,1)} %all-gather.20.cloned.1.call-done, bf16[4,2048,256]{2,1,0:T(8,128)(2,1)} %all-gather.14.cloned.1.call-done, f32[384,256]{1,0:T(8,128)S(1)} %fusion.38), kind=kOutput, calls=%fused_computation.24 | convolution fusion | flops 805896192 | bytes 7208960 | tf_op jit(solution)/shard_map/dot_general | solution.py:114
  228.6 7.3 %add_convert_fusion = bf16[384,2048]{1,0:T(8,128)(2,1)} fusion(f32[384,2048]{1,0:T(8,128)} %fusion.6, f32[384,2048]{1,0:T(8,128)} %fusion.8, f32[384,2048]{1,0:T(8,128)} %fusion.7, bf16[1,1024,2048]{2,1,0:T(8,128)(2,1)} %all-gather.20.cloned.1.call-done, bf16[384,2048]{1,0:T(8,128)(2,1)S(1)} %bitcast.604, ...), kind=kOutput, calls=%fused_computation | convolution fusion | flops 809041920 | bytes 15073280 | tf_op jit(solution)/shard_map/dot_general | solution.py:114
  236.0 4.0 %all-to-all-start.2 = ((bf16[8,48,2048]{2,1,0:T(8,128)(2,1)}), bf16[8,48,2048]{2,1,0:T(8,128)(2,1)S(1)}, u32[]{:S(2)}, u32[]{:S(2)}) async-start(bf16[8,48,2048]{2,1,0:T(8,128)(2,1)} %bitcast.607), calls=%async_computation.2 | async-start | bytes 3145728 | tf_op jit(solution)/shard_map/all_to_all | solution.py:221
  240.1 1.5 fusion.48
  244.5 1.8 fusion.31
  246.3 2.8 convolution_add_fusion.4
  249.1 3.2 %convolution_add_fusion.3 = f32[128,2048]{1,0:T(8,128)} fusion(f32[128,2048]{1,0:T(8,128)} %convolution_add_fusion.4, bf16[512,2048]{1,0:T(8,128)(2,1)} %all-gather.10.cloned.1.call-done, bf16[8192,128]{1,0:T(8,128)(2,1)} %all-gather.18.cloned.1.call-done, f32[128,128]{1,0:T(8,128)S(1)} %fusion.53, bf16[128,2048]{1,0:T(8,128)(2,1)S(1)} %get-tuple-element.6, ...), kind=kOutput, calls=%fused_computation.5 | convolution fusion | flops 135626752 | bytes 3744256 | tf_op jit(solution)/shard_map/dot_general | solution.py:114
  252.3 2.1 convolution_add_fusion.2
  254.4 22.5 %all-to-all-done.2 = bf16[8,48,2048]{2,1,0:T(8,128)(2,1)S(1)} async-done(((bf16[8,48,2048]{2,1,0:T(8,128)(2,1)}), bf16[8,48,2048]{2,1,0:T(8,128)(2,1)S(1)}, u32[]{:S(2)}, u32[]{:S(2)}) %all-to-all-start.2) | async-done | bytes 1572896 | tf_op jit(solution)/shard_map/all_to_all | solution.py:221
  (321 shorter events, 82.1 us)
Async XLA Ops:
  6.5 201.6 %all-gather.12.cloned.1.call-start = ((), (), s32[]{:S(2)}) async-start(), calls=%async_computation.4 | async-start | bytes 5242880 | tf_op jit(solution)/shard_map/all_gather | solution.py:162
  7.3 204.6 %all-gather.14.cloned.1.call-start = ((), (), s32[]{:S(2)}) async-start(), calls=%async_computation.5 | async-start | bytes 5242880 | tf_op jit(solution)/shard_map/all_gather | solution.py:163
  8.0 203.8 %all-gather.20.cloned.1.call-start = ((), (), s32[]{:S(2)}) async-start(), calls=%async_computation.8 | async-start | bytes 5242880 | tf_op jit(solution)/shard_map/all_gather | solution.py:164
  8.7 231.4 %all-gather.16.cloned.1.call-start = ((), (), s32[]{:S(2)}) async-start(), calls=%async_computation.6 | async-start | bytes 2621440 | tf_op jit(solution)/shard_map/all_gather | solution.py:165
  106.2 9.2 %copy-start.26 = (bf16[8,2,8,128]{3,2,1,0:T(8,128)(2,1)S(1)}, bf16[8,2,8,128]{3,2,1,0:T(8,128)(2,1)}, u32[]{:S(2)}) copy-start(bf16[8,2,8,128]{3,2,1,0:T(8,128)(2,1)} %get-tuple-element.22) | copy-start | bytes 98308
  106.2 9.2 %copy-start.48 = (f32[1,2,64]{2,0,1:T(1,128)S(1)}, f32[1,2,64]{2,0,1:T(1,128)}, u32[]{:S(2)}) copy-start(f32[1,2,64]{2,0,1:T(1,128)} %get-tuple-element.55) | copy-start | bytes 1540
  107.5 25.7 %copy-start.4 = (f32[8,64,2,64]{3,1,2,0:T(8,128)}, f32[8,64,2,64]{3,1,2,0:T(8,128)S(1)}, u32[]{:S(2)}) copy-start(f32[8,64,2,64]{3,1,2,0:T(8,128)S(1)} %fusion.65) | copy-start | bytes 786436
  107.5 10.0 %copy-start.25 = (bf16[8,2,8,128]{3,2,1,0:T(8,128)(2,1)S(1)}, bf16[8,2,8,128]{3,2,1,0:T(8,128)(2,1)}, u32[]{:S(2)}) copy-start(bf16[8,2,8,128]{3,2,1,0:T(8,128)(2,1)} %get-tuple-element.21) | copy-start | bytes 98308
  107.5 10.0 %copy-start.47 = (f32[1,2,64]{2,0,1:T(1,128)S(1)}, f32[1,2,64]{2,0,1:T(1,128)}, u32[]{:S(2)}) copy-start(f32[1,2,64]{2,0,1:T(1,128)} %get-tuple-element.54) | copy-start | bytes 1540
  107.5 12.1 %copy-start.24 = (bf16[8,2,8,128]{3,2,1,0:T(8,128)(2,1)S(1)}, bf16[8,2,8,128]{3,2,1,0:T(8,128)(2,1)}, u32[]{:S(2)}) copy-start(bf16[8,2,8,128]{3,2,1,0:T(8,128)(2,1)} %get-tuple-element.20) | copy-start | bytes 98308
  107.6 12.1 %copy-start.46 = (f32[1,2,64]{2,0,1:T(1,128)S(1)}, f32[1,2,64]{2,0,1:T(1,128)}, u32[]{:S(2)}) copy-start(f32[1,2,64]{2,0,1:T(1,128)} %get-tuple-element.53) | copy-start | bytes 1540
  107.6 14.2 %copy-start.23 = (bf16[8,2,8,128]{3,2,1,0:T(8,128)(2,1)S(1)}, bf16[8,2,8,128]{3,2,1,0:T(8,128)(2,1)}, u32[]{:S(2)}) copy-start(bf16[8,2,8,128]{3,2,1,0:T(8,128)(2,1)} %get-tuple-element.25) | copy-start | bytes 98308
  107.6 14.2 %copy-start.45 = (f32[1,2,64]{2,0,1:T(1,128)S(1)}, f32[1,2,64]{2,0,1:T(1,128)}, u32[]{:S(2)}) copy-start(f32[1,2,64]{2,0,1:T(1,128)} %get-tuple-element.52) | copy-start | bytes 1540
  109.8 14.0 %copy-start.22 = (bf16[8,2,8,128]{3,2,1,0:T(8,128)(2,1)S(1)}, bf16[8,2,8,128]{3,2,1,0:T(8,128)(2,1)}, u32[]{:S(2)}) copy-start(bf16[8,2,8,128]{3,2,1,0:T(8,128)(2,1)} %get-tuple-element.19) | copy-start | bytes 98308
  109.8 14.0 %copy-start.44 = (f32[1,2,64]{2,0,1:T(1,128)S(1)}, f32[1,2,64]{2,0,1:T(1,128)}, u32[]{:S(2)}) copy-start(f32[1,2,64]{2,0,1:T(1,128)} %get-tuple-element.51) | copy-start | bytes 1540
  109.8 16.2 %copy-start.52 = (f32[2,64]{1,0:T(2,128)S(1)}, f32[2,64]{1,0:T(2,128)}, u32[]{:S(2)}) copy-start(f32[2,64]{1,0:T(2,128)} %get-tuple-element.36) | copy-start | bytes 1540
  109.8 16.2 %copy-start.53 = (f32[2,64]{1,0:T(2,128)S(1)}, f32[2,64]{1,0:T(2,128)}, u32[]{:S(2)}) copy-start(f32[2,64]{1,0:T(2,128)} %get-tuple-element.37) | copy-start | bytes 1540
  109.8 16.2 %copy-start.54 = (f32[2,64]{1,0:T(2,128)S(1)}, f32[2,64]{1,0:T(2,128)}, u32[]{:S(2)}) copy-start(f32[2,64]{1,0:T(2,128)} %get-tuple-element.38) | copy-start | bytes 1540
  109.8 16.2 %copy-start.55 = (f32[2,64]{1,0:T(2,128)S(1)}, f32[2,64]{1,0:T(2,128)}, u32[]{:S(2)}) copy-start(f32[2,64]{1,0:T(2,128)} %get-tuple-element.39) | copy-start | bytes 1540
  109.8 16.2 %copy-start.56 = (f32[2,64]{1,0:T(2,128)S(1)}, f32[2,64]{1,0:T(2,128)}, u32[]{:S(2)}) copy-start(f32[2,64]{1,0:T(2,128)} %get-tuple-element.40) | copy-start | bytes 1540
  109.9 16.2 %copy-start.57 = (f32[2,64]{1,0:T(2,128)S(1)}, f32[2,64]{1,0:T(2,128)}, u32[]{:S(2)}) copy-start(f32[2,64]{1,0:T(2,128)} %get-tuple-element.41) | copy-start | bytes 1540
  109.9 16.2 %copy-start.58 = (f32[2,64]{1,0:T(2,128)S(1)}, f32[2,64]{1,0:T(2,128)}, u32[]{:S(2)}) copy-start(f32[2,64]{1,0:T(2,128)} %get-tuple-element.42) | copy-start | bytes 1540
  109.9 16.2 %copy-start.59 = (f32[2,64]{1,0:T(2,128)S(1)}, f32[2,64]{1,0:T(2,128)}, u32[]{:S(2)}) copy-start(f32[2,64]{1,0:T(2,128)} %get-tuple-element.43) | copy-start | bytes 1540
  110.2 16.9 %copy-start.7 = (f32[8,64,2,64]{1,3,2,0:T(8,128)S(1)}, f32[8,64,2,64]{1,3,2,0:T(8,128)}, u32[]{:S(2)}) copy-start(f32[8,64,2,64]{1,3,2,0:T(8,128)} %copy.400) | copy-start | bytes 786436
  117.5 9.8 %copy-start.20 = (f32[64,2,128]{2,0,1:T(8,128)S(1)}, f32[64,2,128]{2,0,1:T(8,128)}, u32[]{:S(2)}) copy-start(f32[64,2,128]{2,0,1:T(8,128)} %slice.528) | copy-start | bytes 196612
  117.5 9.8 %copy-start.43 = (f32[1,2,64]{2,0,1:T(1,128)S(1)}, f32[1,2,64]{2,0,1:T(1,128)}, u32[]{:S(2)}) copy-start(f32[1,2,64]{2,0,1:T(1,128)} %get-tuple-element.64) | copy-start | bytes 1540
  134.6 10.7 %copy-start.32 = (f32[8,2,64]{2,0,1:T(8,128)S(1)}, f32[8,2,64]{2,0,1:T(8,128)}, u32[]{:S(2)}) copy-start(f32[8,2,64]{2,0,1:T(8,128)} %get-tuple-element.13) | copy-start | bytes 12292
  150.6 9.4 %all-to-all-start = ((bf16[4,128,256]{2,1,0:T(8,128)(2,1)}), bf16[4,128,256]{2,1,0:T(8,128)(2,1)S(1)}, u32[]{:S(2)}, u32[]{:S(2)}) async-start(bf16[4,128,256]{2,1,0:T(8,128)(2,1)} %bitcast.143), calls=%async_computation | async-start | bytes 524288 | tf_op jit(solution)/shard_map/all_to_all | solution.py:202
  154.0 90.4 %all-gather.10.cloned.1.call-start = ((), (), s32[]{:S(2)}) async-start(), calls=%async_computation.3 | async-start | bytes 2621440 | tf_op jit(solution)/shard_map/all_gather | solution.py:167
  165.8 42.3 %all-to-all-start.1 = ((bf16[8,48,2048]{2,1,0:T(8,128)(2,1)}), bf16[8,48,2048]{2,1,0:T(8,128)(2,1)S(1)}, u32[]{:S(2)}, u32[]{:S(2)}) async-start(bf16[8,48,2048]{2,1,0:T(8,128)(2,1)} %bitcast.608), calls=%async_computation.1 | async-start | bytes 3145728 | tf_op jit(solution)/shard_map/all_to_all | solution.py:210
  171.4 73.0 %all-gather.18.cloned.1.call-start = ((), (), s32[]{:S(2)}) async-start(), calls=%async_computation.7 | async-start | bytes 2621440 | tf_op jit(solution)/shard_map/all_gather | solution.py:166
  236.0 41.0 %all-to-all-start.2 = ((bf16[8,48,2048]{2,1,0:T(8,128)(2,1)}), bf16[8,48,2048]{2,1,0:T(8,128)(2,1)S(1)}, u32[]{:S(2)}, u32[]{:S(2)}) async-start(bf16[8,48,2048]{2,1,0:T(8,128)(2,1)} %bitcast.607), calls=%async_computation.2 | async-start | bytes 3145728 | tf_op jit(solution)/shard_map/all_to_all | solution.py:221
  (50 other events, 235.0 us)
Sparse Core Ops, SparseCore 0:
  8.9 37.2 all-gather.11
  47.7 34.4 all-gather.13
  83.7 34.4 all-gather.19
  119.6 22.5 all-gather.15
  156.1 24.0 all-gather.9
  181.6 22.5 all-gather.17
where the time goes:
time: 288 us; the launch traced here: 286 us
  matrix products  83 us (29%)
  waiting for transfers between devices  66.7 us (23%)
  local copies, waits for them, and re-layouts  42.4 us (15%)
  blocking collectives  33.1 us (11%)
  other arithmetic  32.2 us (11%)
  between operations  15.1 us (5%)
  starting transfers between devices  13.4 us (5%)
    all_to_all x1, waiting for transfers between devices, body(): lax.all_to_all(outgoing.reshape(experts, capacity, model_width), 'sp', sp...  36.1 us
    all_gather x1, blocking collectives, carried_in(): gathered = lax.all_gather(packed, axis).astype(jnp.float32)  33.1 us
    dot_general x8, matrix products, feed_forward(): jnp.dot(hidden, down_mat[group * width:(group + 1) * width], preferred_el...  32.3 us
    all_to_all x1, waiting for transfers between devices, body(): lax.all_to_all(routed_done.reshape(experts, capacity, model_width), 'sp',...  22.5 us
    dot_general x16, matrix products, advance(): jnp.einsum('asu,sun->asn', query_segment, carried_state, precision=TOP_PR...  17.6 us
    another operation x2, other arithmetic, blockwise(): jnp.cumsum(log_decay.reshape(block_count, BLK, head_count, key_width), ax...  14.1 us
    dot_general x14, matrix products, advance(): jnp.einsum('jco,jcm->com', key_segment, value_segment, precision=TOP_PREC...  10.9 us
    slice x17, local copies, waits for them, and re-layouts, blockwise(): lax.scan(advance, start_state, (query_in, key_out, value_blocks, block_de...  9.6 us
  transfers between devices with their start and end apart: 9, of which 3 were waited for; matrix products, arithmetic and copies ran while one was open for 54% of the time, Pallas kernels for 0%

commit v1 on v0

--- a/solution.py
+++ b/solution.py
@@ -199,7 +199,10 @@
     head_mixed = (
         combined.reshape(span_rows, -1) * jax.nn.silu(out_gate.astype(jnp.float32))
     ).astype(jnp.bfloat16)
-    mixed_out = lax.all_to_all(head_mixed, "tp", split_axis=0, concat_axis=1, tiled=True)
+    mixed_out = jnp.concatenate(
+        lax.all_to_all(jnp.stack(jnp.split(head_mixed, lax.axis_size("tp"), axis=0)), "tp", 0, 0),
+        axis=1,
+    )
     projected = jnp.dot(mixed_out, out_proj, preferred_element_type=jnp.float32)
     residual = (stream.astype(jnp.float32) + normalize(projected) * mix_gain).astype(jnp.bfloat16)
     normed = (normalize(residual.astype(jnp.float32)) * ffn_gain).astype(jnp.bfloat16)

time: 288 us -> 291 us (1.010)
  other arithmetic: 32.2 us -> 35.3 us
    dot_general x14, matrix products: 10.9 us -> 14.2 us  [advance(): jnp.einsum('jco,jcm->com', key_segment, value_segment, precision=TOP_PREC...]
    another operation x8 -> x9, other arithmetic: 6.6 us -> 7.35 us
where the time goes in v1:
time: 291 us; the launch traced here: 289 us
  matrix products  81.8 us (28%)
  waiting for transfers between devices  66.8 us (23%)
  local copies, waits for them, and re-layouts  43.4 us (15%)
  other arithmetic  35.3 us (12%)
  blocking collectives  33.1 us (11%)
  between operations  14.9 us (5%)
  starting transfers between devices  13.3 us (5%)
    all_to_all x1, waiting for transfers between devices, body(): lax.all_to_all(outgoing.reshape(experts, capacity, model_width), 'sp', sp...  36.1 us
    all_gather x1, blocking collectives, carried_in(): gathered = lax.all_gather(packed, axis).astype(jnp.float32)  33.1 us
    dot_general x8, matrix products, feed_forward(): jnp.dot(hidden, down_mat[group * width:(group + 1) * width], preferred_el...  32.2 us
    all_to_all x1, waiting for transfers between devices, body(): lax.all_to_all(routed_done.reshape(experts, capacity, model_width), 'sp',...  22.6 us
    dot_general x16, matrix products, advance(): jnp.einsum('asu,sun->asn', query_segment, carried_state, precision=TOP_PR...  14.9 us
    dot_general x14, matrix products, advance(): jnp.einsum('jco,jcm->com', key_segment, value_segment, precision=TOP_PREC...  14.2 us
    another operation x2, other arithmetic, blockwise(): jnp.cumsum(log_decay.reshape(block_count, BLK, head_count, key_width), ax...  14.1 us
    slice x17, local copies, waits for them, and re-layouts, blockwise(): lax.scan(advance, start_state, (query_in, key_out, value_blocks, block_de...  10.6 us
  transfers between devices with their start and end apart: 9, of which 3 were waited for; matrix products, arithmetic and copies ran while one was open for 54% of the time, Pallas kernels for 0%

profile of v1, /device:TPU:0, one launch (start us, length us, event | category | flops | bytes accessed | tf_op | source)
XLA Modules:
  0.0 288.6 jit_solution(9286686377729508864)
XLA Ops:
  11.9 2.4 reduce-window.14
  17.0 2.4 reduce-window.16
  22.3 3.8 %rev.17 = f32[512,2,128]{0,2,1:T(8,128)S(1)} reverse(f32[512,2,128]{0,2,1:T(8,128)} %bitcast.622), dimensions={0} | reverse | bytes 1048576 | tf_op jit(solution)/shard_map/rev | solution.py:192
  26.1 1.3 fusion.30
  29.0 33.1 %all_gather.28 = bf16[8,258,128]{2,1,0:T(8,128)(2,1)S(1)} all-gather(bf16[1,258,128]{2,1,0:T(8,128)(2,1)S(1)} %pad_maximum_fusion.3), channel_id=1, replica_groups=mesh['sp'=8,'tp'=4] {'sp'}, dimensions={0}, use_global_device_ids=true | all-gather | bytes 594432 | tf_op jit(solution)/shard_map/all_gather | solution.py:25
  72.0 3.3 %rev.18 = f32[512,2,64]{0,2,1:T(8,128)} reverse(f32[512,2,64]{0,2,1:T(8,128)} %get-tuple-element.75), dimensions={0} | reverse | bytes 524288 | tf_op jit(solution)/shard_map/rev | solution.py:190
  75.7 13.0 %fusion.218 = f32[8,64,2,64]{3,0,1,2:T(8,128)S(1)} fusion(f32[8,64,2,64]{3,0,1,2:T(8,128)S(1)} %copy.383), kind=kOutput, calls=%fused_computation.399 | output fusion | flops 4128768 | bytes 524288 | tf_op jit(solution)/shard_map/jit(cumsum)/reduce_window_sum | solution.py:67
  98.0 1.2 fusion.69
  99.3 2.3 copy_multiply_fusion.1
  119.9 1.6 fusion.216
  129.6 1.2 fusion.65
  130.9 2.3 copy_multiply_fusion
  153.5 3.4 %all-to-all-start = ((bf16[4,128,256]{1,2,0:T(8,128)(2,1)}), bf16[4,128,256]{1,2,0:T(8,128)(2,1)S(1)}, u32[]{:S(2)}, u32[]{:S(2)}) async-start(bf16[4,128,256]{1,2,0:T(8,128)(2,1)} %pad_maximum_fusion.2), calls=%async_computation | async-start | bytes 524288 | tf_op jit(solution)/shard_map/all_to_all | solution.py:203
  158.4 4.6 %all-to-all-done = bf16[4,128,256]{1,2,0:T(8,128)(2,1)S(1)} async-done(((bf16[4,128,256]{1,2,0:T(8,128)(2,1)}), bf16[4,128,256]{1,2,0:T(8,128)(2,1)S(1)}, u32[]{:S(2)}, u32[]{:S(2)}) %all-to-all-start) | async-done | bytes 262176 | tf_op jit(solution)/shard_map/all_to_all | solution.py:203
  162.9 3.1 %multiply_reduce_fusion.1 = (f32[128]{0:T(128)S(1)}, f32[128,2048]{1,0:T(8,128)S(1)}) fusion(bf16[128,1024]{0,1:T(8,128)(2,1)S(1)} %bitcast.624, bf16[1024,2048]{1,0:T(8,128)(2,1)} %param.28), kind=kOutput, calls=%fused_computation.110 | convolution fusion | flops 537395072 | bytes 5505536 | tf_op jit(solution)/shard_map/dot_general | solution.py:206
  166.7 1.8 convolution_convert_fusion
  168.5 5.5 %all-to-all-start.1 = ((bf16[8,48,2048]{2,1,0:T(8,128)(2,1)}), bf16[8,48,2048]{2,1,0:T(8,128)(2,1)S(1)}, u32[]{:S(2)}, u32[]{:S(2)}) async-start(bf16[8,48,2048]{2,1,0:T(8,128)(2,1)} %bitcast.616), calls=%async_computation.1 | async-start | bytes 3145728 | tf_op jit(solution)/shard_map/all_to_all | solution.py:213
  174.6 36.1 %all-to-all-done.1 = bf16[8,48,2048]{2,1,0:T(8,128)(2,1)S(1)} async-done(((bf16[8,48,2048]{2,1,0:T(8,128)(2,1)}), bf16[8,48,2048]{2,1,0:T(8,128)(2,1)S(1)}, u32[]{:S(2)}, u32[]{:S(2)}) %all-to-all-start.1) | async-done | bytes 1572896 | tf_op jit(solution)/shard_map/all_to_all | solution.py:213
  210.7 1.9 fusion.39
  214.5 5.0 %fusion.7 = f32[384,2048]{1,0:T(8,128)} fusion(bf16[384,2048]{1,0:T(8,128)(2,1)S(1)} %bitcast.608, bf16[1,1024,2048]{2,1,0:T(8,128)(2,1)} %all-gather.20.cloned.1.call-done, bf16[4,2048,256]{2,1,0:T(8,128)(2,1)} %all-gather.14.cloned.1.call-done, f32[384,256]{1,0:T(8,128)S(1)} %fusion.39), kind=kOutput, calls=%fused_computation.25 | convolution fusion | flops 805896192 | bytes 7208960 | tf_op jit(solution)/shard_map/dot_general | solution.py:114
  219.4 1.8 fusion.37
  221.2 5.0 %fusion.8 = f32[384,2048]{1,0:T(8,128)} fusion(bf16[384,2048]{1,0:T(8,128)(2,1)S(1)} %bitcast.610, bf16[1,1024,2048]{2,1,0:T(8,128)(2,1)} %all-gather.20.cloned.1.call-done, bf16[4,2048,256]{2,1,0:T(8,128)(2,1)} %all-gather.14.cloned.1.call-done, f32[384,256]{1,0:T(8,128)S(1)} %fusion.40), kind=kOutput, calls=%fused_computation.26 | convolution fusion | flops 805896192 | bytes 7208960 | tf_op jit(solution)/shard_map/dot_general | solution.py:114
  226.3 5.0 %fusion.6 = f32[384,2048]{1,0:T(8,128)} fusion(bf16[384,2048]{1,0:T(8,128)(2,1)S(1)} %bitcast.611, bf16[1,1024,2048]{2,1,0:T(8,128)(2,1)} %all-gather.20.cloned.1.call-done, bf16[4,2048,256]{2,1,0:T(8,128)(2,1)} %all-gather.14.cloned.1.call-done, f32[384,256]{1,0:T(8,128)S(1)} %fusion.38), kind=kOutput, calls=%fused_computation.24 | convolution fusion | flops 805896192 | bytes 7208960 | tf_op jit(solution)/shard_map/dot_general | solution.py:114
  231.2 7.3 %add_convert_fusion = bf16[384,2048]{1,0:T(8,128)(2,1)} fusion(f32[384,2048]{1,0:T(8,128)} %fusion.6, f32[384,2048]{1,0:T(8,128)} %fusion.8, f32[384,2048]{1,0:T(8,128)} %fusion.7, bf16[1,1024,2048]{2,1,0:T(8,128)(2,1)} %all-gather.20.cloned.1.call-done, bf16[384,2048]{1,0:T(8,128)(2,1)S(1)} %bitcast.612, ...), kind=kOutput, calls=%fused_computation | convolution fusion | flops 809041920 | bytes 15073280 | tf_op jit(solution)/shard_map/dot_general | solution.py:114
  238.6 4.0 %all-to-all-start.2 = ((bf16[8,48,2048]{2,1,0:T(8,128)(2,1)}), bf16[8,48,2048]{2,1,0:T(8,128)(2,1)S(1)}, u32[]{:S(2)}, u32[]{:S(2)}) async-start(bf16[8,48,2048]{2,1,0:T(8,128)(2,1)} %bitcast.615), calls=%async_computation.2 | async-start | bytes 3145728 | tf_op jit(solution)/shard_map/all_to_all | solution.py:224
  242.7 1.5 fusion.48
  244.3 1.4 fusion.53
  247.1 1.8 fusion.31
  248.9 2.8 convolution_add_fusion.4
  251.7 3.1 %convolution_add_fusion.3 = f32[128,2048]{1,0:T(8,128)} fusion(f32[128,2048]{1,0:T(8,128)} %convolution_add_fusion.4, bf16[512,2048]{1,0:T(8,128)(2,1)} %all-gather.10.cloned.1.call-done, bf16[8192,128]{1,0:T(8,128)(2,1)} %all-gather.18.cloned.1.call-done, f32[128,128]{1,0:T(8,128)S(1)} %fusion.53, bf16[128,2048]{1,0:T(8,128)(2,1)S(1)} %get-tuple-element.6, ...), kind=kOutput, calls=%fused_computation.5 | convolution fusion | flops 135626752 | bytes 3744256 | tf_op jit(solution)/shard_map/dot_general | solution.py:114
  254.8 2.1 convolution_add_fusion.2
  257.0 22.6 %all-to-all-done.2 = bf16[8,48,2048]{2,1,0:T(8,128)(2,1)S(1)} async-done(((bf16[8,48,2048]{2,1,0:T(8,128)(2,1)}), bf16[8,48,2048]{2,1,0:T(8,128)(2,1)S(1)}, u32[]{:S(2)}, u32[]{:S(2)}) %all-to-all-start.2) | async-done | bytes 1572896 | tf_op jit(solution)/shard_map/all_to_all | solution.py:224
  (285 shorter events, 85.9 us)
Async XLA Ops:
  6.5 204.2 %all-gather.12.cloned.1.call-start = ((), (), s32[]{:S(2)}) async-start(), calls=%async_computation.4 | async-start | bytes 5242880 | tf_op jit(solution)/shard_map/all_gather | solution.py:162
  7.3 207.2 %all-gather.14.cloned.1.call-start = ((), (), s32[]{:S(2)}) async-start(), calls=%async_computation.5 | async-start | bytes 5242880 | tf_op jit(solution)/shard_map/all_gather | solution.py:163
  8.0 206.4 %all-gather.20.cloned.1.call-start = ((), (), s32[]{:S(2)}) async-start(), calls=%async_computation.8 | async-start | bytes 5242880 | tf_op jit(solution)/shard_map/all_gather | solution.py:164
  8.7 234.0 %all-gather.16.cloned.1.call-start = ((), (), s32[]{:S(2)}) async-start(), calls=%async_computation.6 | async-start | bytes 2621440 | tf_op jit(solution)/shard_map/all_gather | solution.py:165
  98.0 8.1 %copy-start.30 = (bf16[8,2,8,128]{3,2,1,0:T(8,128)(2,1)S(1)}, bf16[8,2,8,128]{3,2,1,0:T(8,128)(2,1)}, u32[]{:S(2)}) copy-start(bf16[8,2,8,128]{3,2,1,0:T(8,128)(2,1)} %get-tuple-element.26) | copy-start | bytes 98308
  99.2 8.9 %copy-start.29 = (bf16[8,2,8,128]{3,2,1,0:T(8,128)(2,1)S(1)}, bf16[8,2,8,128]{3,2,1,0:T(8,128)(2,1)}, u32[]{:S(2)}) copy-start(bf16[8,2,8,128]{3,2,1,0:T(8,128)(2,1)} %get-tuple-element.25) | copy-start | bytes 98308
  99.3 11.0 %copy-start.28 = (bf16[8,2,8,128]{3,2,1,0:T(8,128)(2,1)S(1)}, bf16[8,2,8,128]{3,2,1,0:T(8,128)(2,1)}, u32[]{:S(2)}) copy-start(bf16[8,2,8,128]{3,2,1,0:T(8,128)(2,1)} %get-tuple-element.24) | copy-start | bytes 98308
  99.3 13.0 %copy-start.27 = (bf16[8,2,8,128]{3,2,1,0:T(8,128)(2,1)S(1)}, bf16[8,2,8,128]{3,2,1,0:T(8,128)(2,1)}, u32[]{:S(2)}) copy-start(bf16[8,2,8,128]{3,2,1,0:T(8,128)(2,1)} %get-tuple-element.29) | copy-start | bytes 98308
  101.6 12.8 %copy-start.26 = (bf16[8,2,8,128]{3,2,1,0:T(8,128)(2,1)S(1)}, bf16[8,2,8,128]{3,2,1,0:T(8,128)(2,1)}, u32[]{:S(2)}) copy-start(bf16[8,2,8,128]{3,2,1,0:T(8,128)(2,1)} %get-tuple-element.23) | copy-start | bytes 98308
  101.6 14.9 %copy-start.7 = (f32[8,64,2,64]{3,0,1,2:T(8,128)S(1)}, f32[8,64,2,64]{3,0,1,2:T(8,128)}, u32[]{:S(2)}) copy-start(f32[8,64,2,64]{3,0,1,2:T(8,128)} %copy.352) | copy-start | bytes 786436
  101.6 14.9 %copy-start.9 = (f32[8,64,2,64]{3,0,1,2:T(8,128)S(1)}, f32[8,64,2,64]{3,0,1,2:T(8,128)}, u32[]{:S(2)}) copy-start(f32[8,64,2,64]{3,0,1,2:T(8,128)} %copy.354) | copy-start | bytes 786436
  118.1 9.9 %copy-start.13 = (f32[64,256]{0,1:T(8,128)S(1)}, f32[64,256]{0,1:T(8,128)}, u32[]{:S(2)}) copy-start(f32[64,256]{0,1:T(8,128)} %get-tuple-element.32) | copy-start | bytes 196612
  118.1 10.6 %copy-start.12 = (f32[64,256]{0,1:T(8,128)S(1)}, f32[64,256]{0,1:T(8,128)}, u32[]{:S(2)}) copy-start(f32[64,256]{0,1:T(8,128)} %get-tuple-element.31) | copy-start | bytes 196612
  129.6 7.0 %copy-start.23 = (f32[64,2,128]{2,0,1:T(8,128)S(1)}, f32[64,2,128]{2,0,1:T(8,128)}, u32[]{:S(2)}) copy-start(f32[64,2,128]{2,0,1:T(8,128)} %slice.534) | copy-start | bytes 196612
  129.6 7.0 %copy-start.47 = (f32[1,2,64]{2,0,1:T(1,128)S(1)}, f32[1,2,64]{2,0,1:T(1,128)}, u32[]{:S(2)}) copy-start(f32[1,2,64]{2,0,1:T(1,128)} %get-tuple-element.67) | copy-start | bytes 1540
  129.6 9.0 %copy-start.22 = (f32[64,2,128]{2,0,1:T(8,128)S(1)}, f32[64,2,128]{2,0,1:T(8,128)}, u32[]{:S(2)}) copy-start(f32[64,2,128]{2,0,1:T(8,128)} %slice.540) | copy-start | bytes 196612
  129.6 9.0 %copy-start.46 = (f32[1,2,64]{2,0,1:T(1,128)S(1)}, f32[1,2,64]{2,0,1:T(1,128)}, u32[]{:S(2)}) copy-start(f32[1,2,64]{2,0,1:T(1,128)} %get-tuple-element.66) | copy-start | bytes 1540
  130.9 9.9 %copy-start.21 = (f32[64,2,128]{2,0,1:T(8,128)S(1)}, f32[64,2,128]{2,0,1:T(8,128)}, u32[]{:S(2)}) copy-start(f32[64,2,128]{2,0,1:T(8,128)} %slice.546) | copy-start | bytes 196612
  130.9 9.9 %copy-start.45 = (f32[1,2,64]{2,0,1:T(1,128)S(1)}, f32[1,2,64]{2,0,1:T(1,128)}, u32[]{:S(2)}) copy-start(f32[1,2,64]{2,0,1:T(1,128)} %get-tuple-element.65) | copy-start | bytes 1540
  130.9 12.0 %copy-start.20 = (f32[64,2,128]{2,0,1:T(8,128)S(1)}, f32[64,2,128]{2,0,1:T(8,128)}, u32[]{:S(2)}) copy-start(f32[64,2,128]{2,0,1:T(8,128)} %slice.552) | copy-start | bytes 196612
  130.9 12.0 %copy-start.44 = (f32[1,2,64]{2,0,1:T(1,128)S(1)}, f32[1,2,64]{2,0,1:T(1,128)}, u32[]{:S(2)}) copy-start(f32[1,2,64]{2,0,1:T(1,128)} %get-tuple-element.64) | copy-start | bytes 1540
  130.9 14.1 %copy-start.19 = (f32[64,2,128]{2,0,1:T(8,128)S(1)}, f32[64,2,128]{2,0,1:T(8,128)}, u32[]{:S(2)}) copy-start(f32[64,2,128]{2,0,1:T(8,128)} %slice.558) | copy-start | bytes 196612
  130.9 14.1 %copy-start.43 = (f32[1,2,64]{2,0,1:T(1,128)S(1)}, f32[1,2,64]{2,0,1:T(1,128)}, u32[]{:S(2)}) copy-start(f32[1,2,64]{2,0,1:T(1,128)} %get-tuple-element.63) | copy-start | bytes 1540
  133.2 13.9 %copy-start.42 = (f32[1,2,64]{2,0,1:T(1,128)S(1)}, f32[1,2,64]{2,0,1:T(1,128)}, u32[]{:S(2)}) copy-start(f32[1,2,64]{2,0,1:T(1,128)} %get-tuple-element.62) | copy-start | bytes 1540
  133.2 16.0 %copy-start.6 = (f32[8,64,2,64]{3,0,1,2:T(8,128)S(1)}, f32[8,64,2,64]{3,0,1,2:T(8,128)}, u32[]{:S(2)}) copy-start(f32[8,64,2,64]{3,0,1,2:T(8,128)} %copy.384) | copy-start | bytes 786436
  133.2 16.0 %copy-start.8 = (f32[8,64,2,64]{3,0,1,2:T(8,128)S(1)}, f32[8,64,2,64]{3,0,1,2:T(8,128)}, u32[]{:S(2)}) copy-start(f32[8,64,2,64]{3,0,1,2:T(8,128)} %copy.385) | copy-start | bytes 786436
  133.2 16.0 %copy-start.35 = (f32[8,2,64]{2,0,1:T(8,128)S(1)}, f32[8,2,64]{2,0,1:T(8,128)}, u32[]{:S(2)}) copy-start(f32[8,2,64]{2,0,1:T(8,128)} %get-tuple-element.13) | copy-start | bytes 12292
  153.5 9.4 %all-to-all-start = ((bf16[4,128,256]{1,2,0:T(8,128)(2,1)}), bf16[4,128,256]{1,2,0:T(8,128)(2,1)S(1)}, u32[]{:S(2)}, u32[]{:S(2)}) async-start(bf16[4,128,256]{1,2,0:T(8,128)(2,1)} %pad_maximum_fusion.2), calls=%async_computation | async-start | bytes 524288 | tf_op jit(solution)/shard_map/all_to_all | solution.py:203
  156.9 90.1 %all-gather.10.cloned.1.call-start = ((), (), s32[]{:S(2)}) async-start(), calls=%async_computation.3 | async-start | bytes 2621440 | tf_op jit(solution)/shard_map/all_gather | solution.py:167
  168.5 42.2 %all-to-all-start.1 = ((bf16[8,48,2048]{2,1,0:T(8,128)(2,1)}), bf16[8,48,2048]{2,1,0:T(8,128)(2,1)S(1)}, u32[]{:S(2)}, u32[]{:S(2)}) async-start(bf16[8,48,2048]{2,1,0:T(8,128)(2,1)} %bitcast.616), calls=%async_computation.1 | async-start | bytes 3145728 | tf_op jit(solution)/shard_map/all_to_all | solution.py:213
  174.0 73.1 %all-gather.18.cloned.1.call-start = ((), (), s32[]{:S(2)}) async-start(), calls=%async_computation.7 | async-start | bytes 2621440 | tf_op jit(solution)/shard_map/all_gather | solution.py:166
  238.6 41.0 %all-to-all-start.2 = ((bf16[8,48,2048]{2,1,0:T(8,128)(2,1)}), bf16[8,48,2048]{2,1,0:T(8,128)(2,1)S(1)}, u32[]{:S(2)}, u32[]{:S(2)}) async-start(bf16[8,48,2048]{2,1,0:T(8,128)(2,1)} %bitcast.615), calls=%async_computation.2 | async-start | bytes 3145728 | tf_op jit(solution)/shard_map/all_to_all | solution.py:224
  (32 other events, 116.7 us)
Sparse Core Ops, SparseCore 0:
  8.9 37.2 all-gather.11
  47.7 34.4 all-gather.13
  83.8 34.4 all-gather.19
  119.7 22.5 all-gather.15
  159.0 23.9 all-gather.9
  184.4 22.5 all-gather.17
